TPU v7x, 32 devices: a whole 2x2x4 slice. The times are simulated.
32 devices in a mesh: ep: 8 (over z, x), tp: 4 (over y, core).
Axes of the slice: x: 2, y: 2, z: 4, core: 2. Of those that a mesh axis runs over, the one named last changes fastest.
Arguments:
- queries: bfloat16 [4096, 1024], P('ep', 'tp'), may hold values from -12 to 12
- keys_values: bfloat16 [4096, 8, 128], P('ep', 'tp'), may hold values from -12 to 12
- sink_logits: float32 [16], P('tp'), may hold values from 1 to 7
- out_weight: bfloat16 [1024, 2048], P('tp'), may hold values from -0.5 to 0.5
- expert_input: bfloat16 [4096, 2048], P(('ep', 'tp')), may hold values from -6 to 6
- norm_gain: float32 [2048], replicated, may hold values from 0.1 to 1.9
- route_group: int32 [4096], P(('ep', 'tp')), may hold values from 0 to 3, as said below
- route_expert: int32 [4096, 2], P(('ep', 'tp')), may hold values from 0 to 3, as said below
- group_logits: float32 [4096, 4], P(('ep', 'tp')), may hold values from -6 to 6
- expert_logits: float32 [4096, 2], P(('ep', 'tp')), may hold values from -6 to 6
- gate_weight: bfloat16 [16, 2048, 4096], P('ep', None, 'tp'), may hold values from -0.125 to 0.125
- up_weight: bfloat16 [16, 2048, 4096], P('ep', None, 'tp'), may hold values from -0.125 to 0.125
- down_weight: bfloat16 [16, 4096, 2048], P('ep', 'tp'), may hold values from -0.1875 to 0.1875
Outputs:
- mixed_rows: bfloat16 [4096, 2048], P(('ep', 'tp'))
- expert_mix: bfloat16 [4096, 2048], P(('ep', 'tp'))
Inputs may be any that keep to these rules, and one draw needn't show every extreme that they name: `route_group`: among the 128 tokens of one device, every group is named by the same number of tokens. `route_expert`: A token's 2 entries are different members of the group that route_group names; among the 128 tokens of one device, every expert (group and member) is named exactly 16 times.
All inputs are finite; a program needn't handle non-finite values.
Results may differ from a plain program's by a relative error of at most 0.015.
Values may be sent and summed in bfloat16 or wider, within the bound.
A program may use at most 128 MiB of HBM per device.

v0:
```python
import jax
import jax.numpy as jnp
from jax import lax
from jax.sharding import PartitionSpec as P

HEADS = 16
WINDOW = 128
GROUPS = 4


norm_eps = 1e-06
masked_score = -1e30


def extended(cells, sides, width):
    for axis, dim in sides:
        count = lax.axis_size(axis)
        ends = count - 1
        head = lax.slice_in_dim(cells, 0, width, axis=dim)
        tail = lax.slice_in_dim(cells, cells.shape[dim] - width, cells.shape[dim], axis=dim)
        cells = jnp.concatenate(
            [
                lax.ppermute(tail, axis, [(i, (i + 1) % count) for i in range(ends)]),
                cells,
                lax.ppermute(head, axis, [((i + 1) % count, i) for i in range(ends)]),
            ],
            axis=dim,
        )
    return cells


def normalize(row_block, norm_gain):
    values = row_block.astype(jnp.float32)
    scale = lax.rsqrt(jnp.mean(values * values, axis=-1, keepdims=True) + norm_eps)
    return (values * scale * norm_gain).astype(jnp.bfloat16)


def slot_places(expert_ids, experts, capacity):
    flat_ids = expert_ids.reshape(-1)
    onehot = (flat_ids[:, None] == jnp.arange(experts, dtype=jnp.int32)[None, :]).astype(jnp.int32)
    earlier = jnp.cumsum(onehot, axis=0) - onehot
    return flat_ids * capacity + jnp.sum(onehot * earlier, axis=1)


def arrange(normed, places, slot_count, per_row):
    owners = jnp.repeat(jnp.arange(normed.shape[0], dtype=jnp.int32), per_row)
    table = jnp.zeros((slot_count,), jnp.int32).at[places].set(owners)
    return jnp.take(normed, table, axis=0)


def attend(queries, keys_values, sink_logits):
    row_count = queries.shape[0]
    head_size = keys_values.shape[2] // 2
    kv_local = keys_values.shape[1]
    query_local = queries.shape[1] // head_size
    per_head = query_local // kv_local
    blocks = row_count // WINDOW
    padded = extended(keys_values, (("ep", 0),), WINDOW)
    framed = padded.reshape(blocks + 2, WINDOW, kv_local, 2 * head_size)
    nearby = jnp.concatenate([framed[:-2], framed[1:-1], framed[2:]], axis=1)
    grouped = queries.reshape(blocks, WINDOW, kv_local, per_head, head_size)
    scores = jnp.einsum(
        "nqhgd,nkhd->nhgqk", grouped, nearby[..., :head_size], preferred_element_type=jnp.float32
    ) * head_size ** (-0.5)
    first_row = lax.axis_index("ep") * row_count
    sequence = row_count * lax.axis_size("ep")
    query_place = first_row + jnp.arange(row_count, dtype=jnp.int32).reshape(blocks, WINDOW)
    key_place = (
        first_row
        + jnp.arange(blocks, dtype=jnp.int32)[:, None] * WINDOW
        - WINDOW
        + jnp.arange(3 * WINDOW, dtype=jnp.int32)[None, :]
    )
    distance = jnp.abs(key_place[:, None, :] - query_place[:, :, None])
    allowed = (
        (distance <= WINDOW) & (key_place >= 0)[:, None, :] & (key_place < sequence)[:, None, :]
    )
    head_ids = lax.axis_index("tp") * query_local + jnp.arange(
        query_local, dtype=jnp.int32
    ).reshape(kv_local, per_head)
    slopes = jnp.exp2(-8.0 * (head_ids + 1).astype(jnp.float32) / HEADS)
    scores = scores - slopes[None, :, :, None, None] * distance[:, None, None].astype(jnp.float32)
    scores = jnp.where(allowed[:, None, None], scores, masked_score)
    sink_column = sink_logits.reshape(kv_local, per_head)[None, :, :, None]
    highest = jnp.maximum(jnp.max(scores, axis=-1), sink_column)
    exponent = jnp.exp(scores - highest[..., None])
    denominator = jnp.sum(exponent, axis=-1) + jnp.exp(sink_column - highest)
    weights = (exponent / denominator[..., None]).astype(jnp.bfloat16)
    mixed_part = jnp.einsum(
        "nhgqk,nkhd->nqhgd", weights, nearby[..., head_size:], preferred_element_type=jnp.float32
    )
    return mixed_part.astype(jnp.bfloat16).reshape(row_count, query_local * head_size)


def body(
    queries,
    keys_values,
    sink_logits,
    out_weight,
    expert_input,
    norm_gain,
    route_group,
    route_expert,
    group_logits,
    expert_logits,
    gate_weight,
    up_weight,
    down_weight,
):
    attended = attend(queries, keys_values, sink_logits)
    tp_size = lax.axis_size("tp")
    segment = attended
    mixed_rows = lax.psum_scatter(
        jnp.dot(segment, out_weight, preferred_element_type=jnp.float32).astype(jnp.bfloat16),
        "tp",
        scatter_dimension=0,
        tiled=True,
    )
    ep_size = lax.axis_size("ep")
    token_count = expert_input.shape[0]
    model_width = expert_input.shape[1]
    local_experts = gate_weight.shape[0]
    experts = local_experts * ep_size
    members = experts // GROUPS
    per_token = route_expert.shape[1]
    capacity = token_count * per_token // experts
    slot_count = experts * capacity
    own_places = slot_places(route_group[:, None] * members + route_expert, experts, capacity)
    normed = normalize(expert_input, norm_gain)
    outgoing = arrange(normed, own_places, slot_count, per_token).reshape(
        ep_size, local_experts, capacity, model_width
    )
    arrived = lax.all_to_all(outgoing, "ep", split_axis=0, concat_axis=0, tiled=True)
    segment = lax.all_gather(arrived[None], "tp", axis=0, tiled=True)
    gate_act = jnp.einsum(
        "tsxcd,xdh->tsxch", segment, gate_weight, preferred_element_type=jnp.float32
    )
    up_act = jnp.einsum("tsxcd,xdh->tsxch", segment, up_weight, preferred_element_type=jnp.float32)
    hidden_act = (jax.nn.silu(gate_act) * up_act).astype(jnp.bfloat16)
    flat_hidden = hidden_act.reshape(-1, hidden_act.shape[-1])
    share_rows = flat_hidden.shape[0] // tp_size
    segment = flat_hidden
    segment = segment.reshape(
        lax.axis_size("tp") * share_rows // (local_experts * capacity),
        local_experts,
        capacity,
        segment.shape[-1],
    )
    product = jnp.einsum("mxch,xhd->mxcd", segment, down_weight, preferred_element_type=jnp.float32)
    summed = lax.psum_scatter(
        product.reshape(lax.axis_size("tp") * share_rows, model_width).astype(jnp.bfloat16),
        "tp",
        scatter_dimension=0,
        tiled=True,
    )
    returned = lax.all_to_all(
        summed.reshape(ep_size, local_experts * capacity, model_width),
        "ep",
        split_axis=0,
        concat_axis=0,
        tiled=True,
    )
    results = jnp.take(returned.reshape(slot_count, model_width), own_places, axis=0).reshape(
        token_count, per_token, model_width
    )
    group_exp = jnp.exp(group_logits)
    picked = jnp.sum(
        jnp.where(
            jnp.arange(GROUPS, dtype=jnp.int32)[None, :] == route_group[:, None], group_exp, 0.0
        ),
        axis=1,
    ) / jnp.sum(group_exp, axis=1)
    member_exp = jnp.exp(expert_logits)
    route_weight = member_exp / jnp.sum(member_exp, axis=1, keepdims=True) * picked[:, None]
    expert_mix = jnp.sum(route_weight[:, :, None] * results.astype(jnp.float32), axis=1).astype(
        jnp.bfloat16
    )
    return (mixed_rows, expert_mix)


def solution(mesh):
    placed = (
        P("ep", "tp"),
        P("ep", "tp", None),
        P("tp"),
        P("tp", None),
        P(("ep", "tp"), None),
        P(),
        P(("ep", "tp")),
        P(("ep", "tp"), None),
        P(("ep", "tp"), None),
        P(("ep", "tp"), None),
        P("ep", None, "tp"),
        P("ep", None, "tp"),
        P("ep", "tp", None),
    )
    return jax.shard_map(
        body,
        mesh=mesh,
        in_specs=placed,
        out_specs=(P(("ep", "tp"), None), P(("ep", "tp"), None)),
        check_vma=False,
    )
```

profile of v0, /device:TPU:0, one launch (start us, length us, event | category | flops | bytes accessed | tf_op | source)
XLA Modules:
  0.0 198.3 jit_solution(15773216051338938915)
XLA Ops:
  7.2 0.0 copy-start
  7.2 0.0 all-gather.3.cloned.1.call-start
  7.2 0.7 broadcast_multiply_fusion.1
  8.0 0.7 broadcast_multiply_fusion
  8.6 0.1 copy.85
  8.8 0.1 eq.42
  8.9 0.1 reshape.238
  9.1 0.6 reduce-window.6
  9.6 0.2 slice_reduce_fusion
  9.9 0.1 copy.90
  10.0 0.1 mul.126
  10.1 0.1 reshape.263
  10.3 0.1 fusion.31
  10.4 1.4 scatter_custom_fusion
  11.8 1.2 fusion.19
  13.1 0.1 broadcast_in_dim.72
  13.2 1.2 fusion.21
  14.4 1.4 gather_fusion
  15.8 0.2 broadcast_select_fusion.1
  15.9 32.9 %all_to_all.10 = bf16[8,2,16,2048]{3,2,1,0:T(8,128)(2,1)} all-to-all(bf16[8,2,16,2048]{3,2,1,0:T(8,128)(2,1)S(1)} %broadcast_select_fusion.1), channel_id=1, replica_groups=mesh['ep'=8,'tp'=4] {'ep'}, dimensions={0} | all-to-all | bytes 2097152 | tf_op jit(solution)/shard_map/all_to_all | solution.py:133
  48.9 0.0 all-gather.3.cloned.1.call-update
  48.9 0.0 reduce-scatter.5.cloned.1.call-start
  49.0 33.6 %all-gather.3.cloned.1.call-done = bf16[32,2,16,2048]{3,2,1,0:T(8,128)(2,1)} async-done(((bf16[8,2,16,2048]{3,2,1,0:T(8,128)(2,1)}), bf16[32,2,16,2048]{3,2,1,0:T(8,128)(2,1)}) %all-gather.3.cloned.1.call-update) | async-done | bytes 4194320 | tf_op jit(solution)/shard_map/all_gather | solution.py:134
  82.6 2.7 %copy.91 = bf16[32,2,16,2048]{3,2,0,1:T(8,128)(2,1)S(1)} copy(bf16[32,2,16,2048]{3,2,1,0:T(8,128)(2,1)} %all-gather.3.cloned.1.call-done) | data formatting | bytes 8388608 | tf_op jit(solution)/shard_map/all_gather | solution.py:134
  85.3 9.5 %fusion.2 = f32[2,4,8,16,1024]{4,3,2,1,0:T(8,128)} fusion(bf16[4,8,2,16,2048]{4,3,1,0,2:T(8,128)(2,1)S(1)} %bitcast.100, bf16[2,2048,1024]{2,1,0:T(8,128)(2,1)} %param.24), kind=kOutput, calls=%fused_computation.5 | convolution fusion | flops 4294967296 | bytes 16777216 | tf_op jit(solution)/shard_map/tsxcd,xdh->tsxch/dot_general | solution.py:138
  94.8 6.9 %fusion.6 = bf16[4,8,2,16,1024]{4,3,1,0,2:T(8,128)(2,1)S(1)} fusion(f32[2,4,8,16,1024]{4,3,2,1,0:T(8,128)} %fusion.2, bf16[4,8,2,16,2048]{4,3,1,0,2:T(8,128)(2,1)S(1)} %bitcast.101, bf16[2,2048,1024]{2,1,0:T(8,128)(2,1)S(1)} %bitcast.111), kind=kOutput, calls=%fused_computation.10 | convolution fusion | flops 4301258752 | bytes 18874368 | tf_op jit(solution)/shard_map/tsxcd,xdh->tsxch/dot_general | solution.py:135
  101.8 4.7 %convert_bitcast_fusion = bf16[32,2,16,2048]{3,2,0,1:T(8,128)(2,1)S(1)} fusion(bf16[32,2,16,1024]{3,2,0,1:T(8,128)(2,1)S(1)} %bitcast.114, bf16[2,1024,2048]{2,1,0:T(8,128)(2,1)S(1)} %bitcast.113), kind=kOutput, calls=%fused_computation.16 | convolution fusion | flops 4297064448 | bytes 14680064 | tf_op jit(solution)/shard_map/mxch,xhd->mxcd/dot_general | solution.py:149
  106.5 2.2 %copy.92 = bf16[32,2,16,2048]{3,2,1,0:T(8,128)(2,1)} copy(bf16[32,2,16,2048]{3,2,0,1:T(8,128)(2,1)S(1)} %convert_bitcast_fusion) | data formatting | bytes 8388608 | tf_op jit(solution)/shard_map/convert_element_type | solution.py:151
  108.7 0.0 reduce-scatter.5.cloned.1.call-update
  108.8 0.0 reduce-scatter.3.cloned.1.call-start
  108.8 0.9 copy-done.1
  109.7 3.4 %collective-permute-start = (bf16[128,2,128]{2,0,1:T(8,128)(2,1)S(1)}, bf16[128,2,128]{2,0,1:T(8,128)(2,1)S(1)}, u32[]{:S(2)}, u32[]{:S(2)}) collective-permute-start(bf16[128,2,128]{2,0,1:T(8,128)(2,1)S(1)} %get-tuple-element.8), channel_id=1, source_target_pairs={{0,4},{4,8},{8,12},{12,16},{16,20},{20,24},{24,28},{1,5},{5,9},{9,... | collective-permute-start | bytes 196616 | tf_op jit(solution)/shard_map/ppermute | solution.py:23
  113.1 1.5 collective-permute-start.1
  114.6 0.2 copy.78
  114.8 0.2 reshape.274
  115.1 0.1 max.17
  115.2 0.1 fusion.34
  115.2 0.1 iota_add_fusion
  115.3 1.9 fusion.25
  117.2 0.3 fusion.22
  117.5 0.6 multiply_exponential_fusion
  118.1 1.2 collective-permute-done.1
  119.3 0.1 pad_maximum_fusion.2
  119.3 0.2 copy.77
  119.5 0.2 copy.79
  119.7 0.1 pad_maximum_fusion
  119.8 1.9 fusion.38
  121.8 0.1 broadcast_maximum_fusion
  121.9 0.4 fusion.15
  122.3 0.1 exponential_add_fusion
  122.4 0.7 fusion.18
  123.1 0.2 copy.83
  123.3 2.1 %convolution_convert_fusion = bf16[512,2048]{1,0:T(8,128)(2,1)} fusion(bf16[256,2048]{1,0:T(8,128)(2,1)S(1)} %copy-done, bf16[32,8,4,128]{3,2,1,0:T(4,128)(2,1)S(1)} %bitcast.106), kind=kOutput, calls=%fused_computation.21 | convolution fusion | flops 537919488 | bytes 3407872 | tf_op jit(solution)/shard_map/dot_general | solution.py:114
  125.4 0.0 reduce-scatter.3.cloned.1.call-update
  125.4 28.1 %reduce-scatter.5.cloned.1.call-done = bf16[256,2048]{1,0:T(8,128)(2,1)} async-done(((bf16[1024,2048]{1,0:T(8,128)(2,1)}), bf16[256,2048]{1,0:T(8,128)(2,1)}) %reduce-scatter.5.cloned.1.call-update) | async-done | bytes 1048592 | tf_op jit(solution)/shard_map/reduce_scatter | solution.py:150
  153.6 5.5 %all-to-all-start.1 = ((bf16[8,32,2048]{2,1,0:T(8,128)(2,1)}), bf16[8,32,2048]{2,1,0:T(8,128)(2,1)S(1)}, u32[]{:S(2)}, u32[]{:S(2)}) async-start(bf16[8,32,2048]{2,1,0:T(8,128)(2,1)} %bitcast.104), calls=%async_computation.3 | async-start | bytes 2097152 | tf_op jit(solution)/shard_map/all_to_all | solution.py:156
  159.1 0.1 reduce_sum.72
  159.2 0.1 copy.88
  159.3 0.1 copy.89
  159.5 0.1 copy.84
  159.7 25.1 %all-to-all-done.1 = bf16[8,32,2048]{2,1,0:T(8,128)(2,1)S(1)} async-done(((bf16[8,32,2048]{2,1,0:T(8,128)(2,1)}), bf16[8,32,2048]{2,1,0:T(8,128)(2,1)S(1)}, u32[]{:S(2)}, u32[]{:S(2)}) %all-to-all-start.1) | async-done | bytes 1048608 | tf_op jit(solution)/shard_map/all_to_all | solution.py:156
  184.7 1.4 gather_fusion.1
  186.1 0.7 gather.15
  186.8 4.9 %multiply_reduce_fusion = bf16[128,2048]{1,0:T(8,128)(2,1)} fusion(bf16[128,2,2048]{2,1,0:T(2,128)(2,1)S(1)} %gather.15, pred[128,2]{1,0:T(8,128)(4,1)S(1)} %copy.89, f32[128,2]{1,0:T(8,128)S(1)} %copy.84), kind=kLoop, calls=%fused_computation.23 | loop fusion | flops 1835008 | bytes 1574144 | tf_op jit(solution)/shard_map/reduce_sum | solution.py:175
  (43 shorter events, 0.3 us)
Async XLA Ops:
  7.2 116.1 %copy-start = (bf16[256,2048]{1,0:T(8,128)(2,1)S(1)}, bf16[256,2048]{1,0:T(8,128)(2,1)}, u32[]{:S(2)}) copy-start(bf16[256,2048]{1,0:T(8,128)(2,1)} %param.16) | copy-start | bytes 3145732
  7.2 75.4 %all-gather.3.cloned.1.call-start = ((), (), s32[]{:S(2)}) async-start(), calls=%async_computation.6 | async-start | bytes 5242880 | tf_op jit(solution)/shard_map/all_gather | solution.py:134
  48.9 104.6 %reduce-scatter.5.cloned.1.call-start = ((), (), s32[]{:S(2)}) async-start(), calls=%async_computation.5 | async-start | bytes 5242880 | tf_op jit(solution)/shard_map/reduce_scatter | solution.py:150
  82.6 12.2 %slice-start = ((s8[8388608]{0:T(1024)(128)(4,1)}), s8[4194304]{0:T(1024)(128)(4,1)S(1)}, s32[]{:S(2)}) async-start(s8[8388608]{0:T(1024)(128)(4,1)} %bitcast.110), calls=%async_computation.7 | async-start | bytes 8388608
  85.2 9.6 %slice-start.1 = ((s8[8388608]{0:T(1024)(128)(4,1)}), s8[4194304]{0:T(1024)(128)(4,1)S(1)}, s32[]{:S(2)}) async-start(s8[8388608]{0:T(1024)(128)(4,1)} %bitcast.110), calls=%async_computation.8 | async-start | bytes 8388608
  85.2 16.5 %slice-start.2 = ((s8[8388608]{0:T(1024)(128)(4,1)}), s8[4194304]{0:T(1024)(128)(4,1)S(1)}, s32[]{:S(2)}) async-start(s8[8388608]{0:T(1024)(128)(4,1)} %bitcast.112), calls=%async_computation.9 | async-start | bytes 8388608
  94.8 7.0 %slice-start.3 = ((s8[8388608]{0:T(1024)(128)(4,1)}), s8[4194304]{0:T(1024)(128)(4,1)S(1)}, s32[]{:S(2)}) async-start(s8[8388608]{0:T(1024)(128)(4,1)} %bitcast.112), calls=%async_computation.10 | async-start | bytes 8388608
  108.7 0.9 copy-start.1
  108.7 6.1 %copy-start.2 = (bf16[512,256]{1,0:T(8,128)(2,1)S(1)}, bf16[512,256]{1,0:T(8,128)(2,1)}, u32[]{:S(2)}) copy-start(bf16[512,256]{1,0:T(8,128)(2,1)} %param.13) | copy-start | bytes 786436
  108.7 6.3 %copy-start.6 = (f32[4]{0:T(128)S(1)}, f32[4]{0:T(128)}, u32[]{:S(2)}) copy-start(f32[4]{0:T(128)} %param.15) | copy-start | bytes 52
  108.8 83.0 %reduce-scatter.3.cloned.1.call-start = ((), (), s32[]{:S(2)}) async-start(), calls=%async_computation.4 | async-start | bytes 2621440 | tf_op jit(solution)/shard_map/reduce_scatter | solution.py:113
  109.7 8.3 %collective-permute-start = (bf16[128,2,128]{2,0,1:T(8,128)(2,1)S(1)}, bf16[128,2,128]{2,0,1:T(8,128)(2,1)S(1)}, u32[]{:S(2)}, u32[]{:S(2)}) collective-permute-start(bf16[128,2,128]{2,0,1:T(8,128)(2,1)S(1)} %get-tuple-element.8), channel_id=1, source_target_pairs={{0,4},{4,8},{8,12},{12,16},{16,20},{20,24},{24,28},{1,5},{5,9},{9,... | collective-permute-start | bytes 196616 | tf_op jit(solution)/shard_map/ppermute | solution.py:23
  113.1 6.2 %collective-permute-start.1 = (bf16[128,2,128]{2,0,1:T(8,128)(2,1)S(1)}, bf16[128,2,128]{2,0,1:T(8,128)(2,1)S(1)}, u32[]{:S(2)}, u32[]{:S(2)}) collective-permute-start(bf16[128,2,128]{2,0,1:T(8,128)(2,1)S(1)} %get-tuple-element.9), channel_id=1, source_target_pairs={{4,0},{8,4},{12,8},{16,12},{20,16},{24,20},{28,24},{5,1},{9,5},{13... | collective-permute-start | bytes 196616 | tf_op jit(solution)/shard_map/ppermute | solution.py:25
  123.3 36.1 %copy-start.3 = (f32[128,4]{0,1:T(4,128)S(1)}, f32[128,4]{0,1:T(4,128)}, u32[]{:S(2)}) copy-start(f32[128,4]{0,1:T(4,128)} %param.21) | copy-start | bytes 6148
  123.3 36.1 %copy-start.5 = (s32[128]{0:T(128)S(1)}, s32[128]{0:T(128)}, u32[]{:S(2)}) copy-start(s32[128]{0:T(128)} %param.19) | copy-start | bytes 1540
  123.3 36.2 %copy-start.4 = (f32[128,2]{0,1:T(2,128)S(1)}, f32[128,2]{0,1:T(2,128)}, u32[]{:S(2)}) copy-start(f32[128,2]{0,1:T(2,128)} %param.22) | copy-start | bytes 3076
  153.6 31.2 %all-to-all-start.1 = ((bf16[8,32,2048]{2,1,0:T(8,128)(2,1)}), bf16[8,32,2048]{2,1,0:T(8,128)(2,1)S(1)}, u32[]{:S(2)}, u32[]{:S(2)}) async-start(bf16[8,32,2048]{2,1,0:T(8,128)(2,1)} %bitcast.104), calls=%async_computation.3 | async-start | bytes 2097152 | tf_op jit(solution)/shard_map/all_to_all | solution.py:156
Sparse Core Ops, SparseCore 0:
  49.0 33.4 all-gather.2
  108.9 44.6 reduce-scatter.4
  156.7 31.1 reduce-scatter.2
where the time goes:
time: 199 us; the launch traced here: 198 us
  waiting for transfers between devices  88 us (44%)
  blocking collectives  32.9 us (17%)
  matrix products  25.9 us (13%)
  between operations  14.1 us (7%)
  other arithmetic  13.5 us (7%)
  local copies, waits for them, and re-layouts  13.3 us (7%)
  starting transfers between devices  10.5 us (5%)
    all_gather x1, waiting for transfers between devices, body(): segment = lax.all_gather(arrived[None], 'tp', axis=0, tiled=True)  33.6 us
    all_to_all x1, blocking collectives, body(): lax.all_to_all(outgoing, 'ep', split_axis=0, concat_axis=0, tiled=True)  32.9 us
    reduce_scatter x1, waiting for transfers between devices, body(): lax.psum_scatter(product.reshape(lax.axis_size('tp') * share_rows, model_...  28.1 us
    all_to_all x1, waiting for transfers between devices, body(): lax.all_to_all(summed.reshape(ep_size, local_experts * capacity, model_wi...  25.1 us
    dot_general x1, matrix products, body(): jnp.einsum('tsxcd,xdh->tsxch', segment, up_weight, preferred_element_type...  9.53 us
    dot_general x1, matrix products, body(): jnp.einsum('tsxcd,xdh->tsxch', segment, gate_weight, preferred_element_ty...  6.94 us
    all_to_all x1, starting transfers between devices, body(): lax.all_to_all(summed.reshape(ep_size, local_experts * capacity, model_wi...  5.51 us
    reduce_sum x1, other arithmetic, body(): jnp.sum(route_weight[:, :, None] * results.astype(jnp.float32), axis=1)  4.92 us
  transfers between devices with their start and end apart: 6, of which 4 were waited for; matrix products, arithmetic and copies ran while one was open for 9% of the time, Pallas kernels for 0%

commit v1 on v0

v1 whole, which is shorter than its diff:
```python
import jax
import jax.numpy as jnp
from jax import lax
from jax.experimental import pallas as pl
from jax.experimental.pallas import tpu as pltpu
from jax.sharding import PartitionSpec as P
import functools

HEADS = 16
WINDOW = 128
GROUPS = 4


norm_eps = 1e-06
masked_score = -1e30


def extended(cells, sides, width):
    for axis, dim in sides:
        count = lax.axis_size(axis)
        ends = count - 1
        head = lax.slice_in_dim(cells, 0, width, axis=dim)
        tail = lax.slice_in_dim(cells, cells.shape[dim] - width, cells.shape[dim], axis=dim)
        cells = jnp.concatenate(
            [
                lax.ppermute(tail, axis, [(i, (i + 1) % count) for i in range(ends)]),
                cells,
                lax.ppermute(head, axis, [((i + 1) % count, i) for i in range(ends)]),
            ],
            axis=dim,
        )
    return cells


MESH = pl.DeviceIdType.MESH
CORES = 2
META = 128
HI = 32
LO = 64


def expert_kernel(
    dims, x_ref, gain_ref, sel_ref, meta_ref, wg_hbm, wu_hbm, wd_hbm, out_ref,
    wg, wu, wd, sbuf, buf, cbuf, xbuf, hbuf, wrow, pbuf, fb, sb, fin, ret,
    wsem, lsem, zs, zr, gs, gr, ps, pr, fs, fr, ss, sr, bs, br,
):
    planes, ranks, rows, per_block = dims
    tokens, width = x_ref.shape
    local = wg.shape[0]
    units = wg.shape[2]
    per_group = tokens // planes
    sides = rows
    ep, tp = lax.axis_index("ep"), lax.axis_index("tp")
    g, x = ep // ranks, ep % ranks
    y, c = tp // CORES, tp % CORES
    other = 1 - c
    part = pl.ds(0, width)

    def device(g_, x_, y_, c_):
        return (g_ * ranks + x_, y_ * CORES + c_)

    def x_peer(i):
        return lax.rem(x + i, ranks)

    def y_peer(j):
        return lax.rem(y + j, sides)

    loads = []
    for k, (h, v) in enumerate(((wg_hbm, wg), (wu_hbm, wu), (wd_hbm, wd))):
        cp = pltpu.make_async_copy(h, v, wsem.at[k])
        cp.start()
        loads.append(cp)

    barrier = pltpu.get_barrier_semaphore()
    friends = [device(lax.rem(g + d, planes), x, y, c) for d in range(1, planes)]
    friends += [device(g, x_peer(i), y, c) for i in range(1, ranks)]
    friends += [device(g, x, y_peer(j), c) for j in range(1, sides)]
    friends += [device(g, x, y, other)]
    for f in friends:
        pl.semaphore_signal(barrier, inc=1, device_id=f, device_id_type=MESH)

    values = x_ref[...].astype(jnp.float32)
    scale = lax.rsqrt(jnp.mean(values * values, axis=-1, keepdims=True) + norm_eps)
    normed = (values * scale * gain_ref[...]).astype(jnp.bfloat16)
    sel = sel_ref[...]
    ordered = jnp.dot(sel, normed, preferred_element_type=jnp.float32).astype(jnp.bfloat16)
    sbuf[:, :, :width] = ordered.reshape(planes, per_group, width)
    extra = jnp.dot(sel, meta_ref[...], preferred_element_type=jnp.float32).astype(jnp.bfloat16)
    sbuf[:, :, width:] = extra.reshape(planes, per_group, META)

    pl.semaphore_wait(barrier, len(friends))

    def remote(src, dst, s, r, dev):
        cp = pltpu.make_async_remote_copy(
            src_ref=src, dst_ref=dst, send_sem=s, recv_sem=r, device_id=dev, device_id_type=MESH
        )
        cp.start()
        return cp

    sent = []
    for d in range(1, planes):
        to = lax.rem(g + d, planes)
        sent.append(
            remote(sbuf.at[to], buf.at[d, c, x, y], zs.at[d], zr.at[d], device(to, x, y, c))
        )
    own = pltpu.make_async_copy(sbuf.at[g], buf.at[0, c, x, y], lsem)
    own.start()
    own.wait()

    counter = [0]

    def pass_on(d, bx, by, dev):
        block = buf.at[d, c, bx, by]
        sent.append(remote(block, block, gs.at[counter[0]], gr.at[d, c, bx, by], dev))
        counter[0] += 1

    def landed(d, bc, bx, by):
        block = buf.at[d, bc, bx, by]
        pltpu.make_async_remote_copy(
            src_ref=block, dst_ref=block, send_sem=gs.at[0], recv_sem=gr.at[d, bc, bx, by],
            device_id=device(g, x, y, other), device_id_type=MESH,
        ).wait_recv()

    def to_x(d, bx, by):
        for i in range(1, ranks):
            pass_on(d, bx, by, device(g, x_peer(i), y, c))

    def to_y(d, bx, by):
        for j in range(1, sides):
            pass_on(d, bx, by, device(g, x, y_peer(j), c))

    def to_core(d, bx, by):
        pass_on(d, bx, by, device(g, x, y, other))

    def spread(d):
        if d > 0:
            sent[d - 1].wait_recv()
        to_x(d, x, y)
        to_y(d, x, y)
        to_core(d, x, y)

    def relay(d):
        for i in range(1, ranks):
            landed(d, c, x_peer(i), y)
            if d % 2 == 0:
                to_y(d, x_peer(i), y)
            to_core(d, x_peer(i), y)
        for j in range(1, sides):
            landed(d, c, x, y_peer(j))
            if d % 2 == 1:
                to_x(d, x, y_peer(j))
            to_core(d, x, y_peer(j))

    def relay_far(d):
        for i in range(1, ranks):
            for j in range(1, sides):
                landed(d, c, x_peer(i), y_peer(j))
                to_core(d, x_peer(i), y_peer(j))

    def complete(d):
        for bx in range(ranks):
            for by in range(sides):
                landed(d, other, bx, by)

    spread(0)
    for d in range(1, planes):
        spread(d)
        relay(d - 1)
        if d > 1:
            relay_far(d - 2)
    relay(planes - 1)
    relay_far(planes - 2)
    relay_far(planes - 1)
    for d in range(planes):
        complete(d)
    for cp in sent:
        cp.wait_send()
    for cp in loads:
        cp.wait()

    count = CORES * ranks * sides
    many = count * per_group
    slots = count * per_block
    stage = 2

    def gather_rows(first):
        ri = lax.broadcasted_iota(jnp.int32, (many, many), 0)
        ci = lax.broadcasted_iota(jnp.int32, (many, many), 1)
        lower = ((ci < ri) & (ci // per_group == ri // per_group)).astype(jnp.bfloat16)
        lane = lax.broadcasted_iota(jnp.int32, (many, META), 1)
        base = lax.broadcasted_iota(jnp.int32, (many, 1), 0) // per_group * per_block
        slot = lax.broadcasted_iota(jnp.int32, (many, slots), 1).astype(jnp.float32)
        lane_r = lax.broadcasted_iota(jnp.int32, (slots, META), 1)
        for s in range(stage):
            block = buf[first + s].reshape(many, width + META)
            marks = block[:, width:]
            ranks_in = jnp.dot(lower, marks, preferred_element_type=jnp.float32)
            for e in range(local):
                member = x * local + e
                mine = lane == member
                chosen = jnp.sum(jnp.where(mine, marks.astype(jnp.float32), 0.0), axis=1, keepdims=True)
                place = jnp.sum(jnp.where(mine, ranks_in, 0.0), axis=1, keepdims=True)
                place = place + base.astype(jnp.float32)
                hot = jnp.where((place == slot) & (chosen > 0.5), 1.0, 0.0).astype(jnp.bfloat16)
                cbuf[s, e] = hot
                picked = lax.dot_general(
                    hot, block, (((0,), (0,)), ((), ())), preferred_element_type=jnp.float32
                )
                xbuf[e, pl.ds(s * slots, slots), :] = picked[:, :width].astype(jnp.bfloat16)
                tail = picked[:, width:]
                weight = jnp.sum(
                    jnp.where((lane_r == member + HI) | (lane_r == member + LO), tail, 0.0),
                    axis=1, keepdims=True,
                )
                wrow[e, pl.ds(s * slots, slots), :] = jnp.broadcast_to(weight, (slots, META))

    tile = 256

    def hidden_of(e):
        @pl.loop(0, units // tile)
        def _(k):
            cols = pl.ds(pl.multiple_of(k * tile, tile), tile)
            xs = xbuf[e]
            a = jnp.dot(xs, wg[e, :, cols], preferred_element_type=jnp.float32)
            b = jnp.dot(xs, wu[e, :, cols], preferred_element_type=jnp.float32)
            act = a / (1.0 + jnp.exp(-a)) * b * wrow[e, :, :1]
            hbuf[e, :, cols] = act.astype(jnp.bfloat16)

    def project(first):
        @pl.loop(0, width // tile)
        def _(k):
            cols = pl.ds(pl.multiple_of(k * tile, tile), tile)
            outs = [
                jnp.dot(hbuf[e], wd[e, :, cols], preferred_element_type=jnp.float32).astype(jnp.bfloat16)
                for e in range(local)
            ]
            for s in range(stage):
                total = jnp.zeros((many, tile), jnp.float32)
                for e in range(local):
                    total += jnp.dot(
                        cbuf[s, e], outs[e][s * slots : (s + 1) * slots],
                        preferred_element_type=jnp.float32,
                    )
                buf[first + s, :, :, :, :, cols] = total.astype(jnp.bfloat16).reshape(
                    CORES, ranks, sides, per_group, tile
                )

    back = []
    pair, first_hop, second_hop, home = {}, {}, {}, {}

    def swap_cores(d):
        pair[d] = remote(
            buf.at[d, other, :, :, :, part], pbuf.at[d], ps.at[d], pr.at[d], device(g, x, y, other)
        )

    def hop_one(d):
        pair[d].wait_recv()
        for bx in range(ranks):
            for by in range(sides):
                buf[d, c, bx, by, :, part] = (
                    buf[d, c, bx, by, :, part].astype(jnp.float32) + pbuf[d, bx, by].astype(jnp.float32)
                ).astype(jnp.bfloat16)
        first_hop[d] = []
        along_y = d % 2 == 0
        for j in range(1, sides if along_y else ranks):
            for q in range(ranks if along_y else sides):
                if along_y:
                    src, dev = buf.at[d, c, q, y_peer(j), :, part], device(g, x, y_peer(j), c)
                else:
                    src, dev = buf.at[d, c, x_peer(j), q, :, part], device(g, x_peer(j), y, c)
                first_hop[d].append(
                    remote(src, fb.at[d, j - 1, q], fs.at[d, j - 1, q], fr.at[d, j - 1, q], dev)
                )

    def hop_two(d):
        for cp in first_hop[d]:
            cp.wait_recv()
        along_y = d % 2 == 0
        for q in range(ranks if along_y else sides):
            here = (d, c, q, y) if along_y else (d, c, x, q)
            total = buf[(*here, slice(None), part)].astype(jnp.float32)
            for j in range(1, sides if along_y else ranks):
                total += fb[d, j - 1, q].astype(jnp.float32)
            buf[(*here, slice(None), part)] = total.astype(jnp.bfloat16)
        second_hop[d] = []
        for i in range(1, ranks if along_y else sides):
            if along_y:
                src, dev = buf.at[d, c, x_peer(i), y, :, part], device(g, x_peer(i), y, c)
            else:
                src, dev = buf.at[d, c, x, y_peer(i), :, part], device(g, x, y_peer(i), c)
            second_hop[d].append(remote(src, sb.at[d, i - 1], ss.at[d, i - 1], sr.at[d, i - 1], dev))

    def go_home(d):
        for cp in second_hop[d]:
            cp.wait_recv()
        total = buf[d, c, x, y, :, part].astype(jnp.float32)
        for i in range(len(second_hop[d])):
            total += sb[d, i].astype(jnp.float32)
        if d == 0:
            ret[g] = total.astype(jnp.bfloat16)
        else:
            fin[d] = total.astype(jnp.bfloat16)
            to = lax.rem(g + planes - d, planes)
            home[d] = remote(fin.at[d], ret.at[g], bs.at[d], br.at[d], device(to, x, y, c))

    for first in range(0, planes, stage):
        ds = range(first, first + stage)
        before = range(first - stage, first) if first else ()
        gather_rows(first)
        for d in before:
            hop_one(d)
        for e in range(local):
            hidden_of(e)
            if e == 0:
                for d in before:
                    hop_two(d)
        for d in before:
            go_home(d)
        project(first)
        for d in ds:
            swap_cores(d)
    for d in ds:
        hop_one(d)
    for d in ds:
        hop_two(d)
    for d in ds:
        go_home(d)
    for d in range(planes):
        pair[d].wait_send()
        for cp in first_hop[d] + second_hop[d]:
            cp.wait_send()
    for d in range(1, planes):
        home[d].wait_send()
        came = lax.rem(g + d, planes)
        pltpu.make_async_remote_copy(
            src_ref=fin.at[d], dst_ref=ret.at[came], send_sem=bs.at[d], recv_sem=br.at[d],
            device_id=device(came, x, y, c), device_id_type=MESH,
        ).wait_recv()
    out_ref[...] = lax.dot_general(
        sel_ref[...], ret[...].reshape(tokens, width), (((0,), (0,)), ((), ())),
        preferred_element_type=jnp.float32,
    ).astype(jnp.bfloat16)


def expert_mix_of(
    expert_input, norm_gain, route_group, route_expert, group_logits, expert_logits,
    gate_weight, up_weight, down_weight,
):
    ep_size, tp_size = lax.axis_size("ep"), lax.axis_size("tp")
    tokens, width = expert_input.shape
    local, _, units = gate_weight.shape
    planes, ranks, sides = GROUPS, ep_size // GROUPS, tp_size // CORES
    members = local * ranks
    per_group = tokens // planes
    chosen = route_expert.shape[1]
    per_block = per_group * chosen // members
    slots = CORES * ranks * sides * per_block
    many = CORES * ranks * sides * per_group
    ids = jnp.arange(tokens, dtype=jnp.int32)
    same = (route_group[:, None] == route_group[None, :]) & (ids[:, None] < ids[None, :])
    place = route_group * per_group + jnp.sum(same.astype(jnp.int32), axis=0)
    sel = (place[None, :] == ids[:, None]).astype(jnp.bfloat16)
    group_exp = jnp.exp(group_logits)
    groups = jnp.arange(GROUPS, dtype=jnp.int32)[None, :]
    picked = jnp.sum(jnp.where(groups == route_group[:, None], group_exp, 0.0), axis=1) / jnp.sum(
        group_exp, axis=1
    )
    member_exp = jnp.exp(expert_logits)
    weight = member_exp / jnp.sum(member_exp, axis=1, keepdims=True) * picked[:, None]
    high = lax.reduce_precision(weight, 8, 7)
    low = weight - high
    lane = jnp.arange(META, dtype=jnp.int32)[None, :]
    meta = jnp.zeros((tokens, META), jnp.float32)
    for k in range(chosen):
        at = route_expert[:, k : k + 1]
        meta = meta + jnp.where(lane == at, 1.0, 0.0)
        meta = meta + jnp.where(lane == at + HI, high[:, k : k + 1], 0.0)
        meta = meta + jnp.where(lane == at + LO, low[:, k : k + 1], 0.0)
    bf16, dma = jnp.bfloat16, pltpu.SemaphoreType.DMA
    most, wide = max(ranks, sides), max(ranks, sides, 2) - 1
    sends = planes * (ranks * sides * 3)
    vmem = pl.BlockSpec(memory_space=pltpu.VMEM)
    hbm = pl.BlockSpec(memory_space=pl.ANY)
    rows = 2 * slots
    return pl.pallas_call(
        functools.partial(expert_kernel, (planes, ranks, sides, per_block)),
        out_shape=jax.ShapeDtypeStruct((tokens, width), bf16),
        in_specs=[vmem] * 4 + [hbm] * 3,
        out_specs=vmem,
        scratch_shapes=[
            pltpu.VMEM(gate_weight.shape, bf16),
            pltpu.VMEM(up_weight.shape, bf16),
            pltpu.VMEM(down_weight.shape, bf16),
            pltpu.VMEM((planes, per_group, width + META), bf16),
            pltpu.VMEM((planes, CORES, ranks, sides, per_group, width + META), bf16),
            pltpu.VMEM((2, local, many, slots), bf16),
            pltpu.VMEM((local, rows, width), bf16),
            pltpu.VMEM((local, rows, units), bf16),
            pltpu.VMEM((local, rows, META), jnp.float32),
            pltpu.VMEM((planes, ranks, sides, per_group, width), bf16),
            pltpu.VMEM((planes, wide, most, per_group, width), bf16),
            pltpu.VMEM((planes, wide, per_group, width), bf16),
            pltpu.VMEM((planes, per_group, width), bf16),
            pltpu.VMEM((planes, per_group, width), bf16),
            dma((3,)), dma,
            dma((planes,)), dma((planes,)),
            dma((sends,)), dma((planes, CORES, ranks, sides)),
            dma((planes,)), dma((planes,)),
            dma((planes, wide, most)), dma((planes, wide, most)),
            dma((planes, wide)), dma((planes, wide)),
            dma((planes,)), dma((planes,)),
        ],
        compiler_params=pltpu.CompilerParams(
            collective_id=0, has_side_effects=True, vmem_limit_bytes=KERNEL_VMEM
        ),
        cost_estimate=pl.CostEstimate(
            flops=6 * 2 * rows * local * width * units, bytes_accessed=6 * local * width * units, transcendentals=0
        ),
    )(expert_input, norm_gain[None, :], sel, meta.astype(bf16), gate_weight, up_weight, down_weight)


KERNEL_VMEM = 66_000_000


def attend(queries, keys_values, sink_logits):
    row_count = queries.shape[0]
    head_size = keys_values.shape[2] // 2
    kv_local = keys_values.shape[1]
    query_local = queries.shape[1] // head_size
    per_head = query_local // kv_local
    blocks = row_count // WINDOW
    padded = extended(keys_values, (("ep", 0),), WINDOW)
    framed = padded.reshape(blocks + 2, WINDOW, kv_local, 2 * head_size)
    nearby = jnp.concatenate([framed[:-2], framed[1:-1], framed[2:]], axis=1)
    grouped = queries.reshape(blocks, WINDOW, kv_local, per_head, head_size)
    scores = jnp.einsum(
        "nqhgd,nkhd->nhgqk", grouped, nearby[..., :head_size], preferred_element_type=jnp.float32
    ) * head_size ** (-0.5)
    first_row = lax.axis_index("ep") * row_count
    sequence = row_count * lax.axis_size("ep")
    query_place = first_row + jnp.arange(row_count, dtype=jnp.int32).reshape(blocks, WINDOW)
    key_place = (
        first_row
        + jnp.arange(blocks, dtype=jnp.int32)[:, None] * WINDOW
        - WINDOW
        + jnp.arange(3 * WINDOW, dtype=jnp.int32)[None, :]
    )
    distance = jnp.abs(key_place[:, None, :] - query_place[:, :, None])
    allowed = (
        (distance <= WINDOW) & (key_place >= 0)[:, None, :] & (key_place < sequence)[:, None, :]
    )
    head_ids = lax.axis_index("tp") * query_local + jnp.arange(
        query_local, dtype=jnp.int32
    ).reshape(kv_local, per_head)
    slopes = jnp.exp2(-8.0 * (head_ids + 1).astype(jnp.float32) / HEADS)
    scores = scores - slopes[None, :, :, None, None] * distance[:, None, None].astype(jnp.float32)
    scores = jnp.where(allowed[:, None, None], scores, masked_score)
    sink_column = sink_logits.reshape(kv_local, per_head)[None, :, :, None]
    highest = jnp.maximum(jnp.max(scores, axis=-1), sink_column)
    exponent = jnp.exp(scores - highest[..., None])
    denominator = jnp.sum(exponent, axis=-1) + jnp.exp(sink_column - highest)
    weights = (exponent / denominator[..., None]).astype(jnp.bfloat16)
    mixed_part = jnp.einsum(
        "nhgqk,nkhd->nqhgd", weights, nearby[..., head_size:], preferred_element_type=jnp.float32
    )
    return mixed_part.astype(jnp.bfloat16).reshape(row_count, query_local * head_size)


def body(
    queries,
    keys_values,
    sink_logits,
    out_weight,
    expert_input,
    norm_gain,
    route_group,
    route_expert,
    group_logits,
    expert_logits,
    gate_weight,
    up_weight,
    down_weight,
):
    attended = attend(queries, keys_values, sink_logits)
    segment = attended
    mixed_rows = lax.psum_scatter(
        jnp.dot(segment, out_weight, preferred_element_type=jnp.float32).astype(jnp.bfloat16),
        "tp",
        scatter_dimension=0,
        tiled=True,
    )
    expert_mix = expert_mix_of(
        expert_input, norm_gain, route_group, route_expert, group_logits, expert_logits,
        gate_weight, up_weight, down_weight,
    )
    return (mixed_rows, expert_mix)


def solution(mesh):
    placed = (
        P("ep", "tp"),
        P("ep", "tp", None),
        P("tp"),
        P("tp", None),
        P(("ep", "tp"), None),
        P(),
        P(("ep", "tp")),
        P(("ep", "tp"), None),
        P(("ep", "tp"), None),
        P(("ep", "tp"), None),
        P("ep", None, "tp"),
        P("ep", None, "tp"),
        P("ep", "tp", None),
    )
    return jax.shard_map(
        body,
        mesh=mesh,
        in_specs=placed,
        out_specs=(P(("ep", "tp"), None), P(("ep", "tp"), None)),
        check_vma=False,
    )
```

time: 199 us -> 136 us (0.68)
  Pallas kernels: 0 us -> 100 us
  waiting for transfers between devices: 88 us -> 0.35 us
  blocking collectives: 32.9 us -> 0 us
  matrix products: 25.9 us -> 3.76 us
  other arithmetic: 13.5 us -> 3.79 us
  local copies, waits for them, and re-layouts: 13.3 us -> 6.84 us
  starting transfers between devices: 10.5 us -> 6.2 us
    pallas_call x0 -> x1, Pallas kernels: none -> 100 us  [expert_mix_of(): pl.pallas_call(functools.partial(expert_kernel, (planes, ranks, sides, pe...]
    all_gather x1 -> x0, waiting for transfers between devices: 33.6 us -> none  [body(): segment = lax.all_gather(arrived[None], 'tp', axis=0, tiled=True)]
    all_to_all x1 -> x0, blocking collectives: 32.9 us -> none  [body(): lax.all_to_all(outgoing, 'ep', split_axis=0, concat_axis=0, tiled=True)]
    reduce_scatter x1 -> x0, waiting for transfers between devices: 28.1 us -> none  [body(): lax.psum_scatter(product.reshape(lax.axis_size('tp') * share_rows, model_...]
    all_to_all x1 -> x0, waiting for transfers between devices: 25.1 us -> none  [body(): lax.all_to_all(summed.reshape(ep_size, local_experts * capacity, model_wi...]
    dot_general x3 -> x0, matrix products: 21.2 us -> none  [the longest x1 9.53 us: body(): jnp.einsum('tsxcd,xdh->tsxch', segment, up_weight, preferred_element_type...]
    reduce_sum x5 -> x3, other arithmetic: 6.28 us -> 0.14 us  [the longest x1 0.1 us: expert_mix_of(): place = route_group * per_group + jnp.sum(same.astype(jnp.int32), axis=0)]
    all_to_all x1 -> x0, starting transfers between devices: 5.51 us -> none  [body(): lax.all_to_all(summed.reshape(ep_size, local_experts * capacity, model_wi...]
  transfers between devices with their start and end apart: 6 -> 3, of which waited for: 4 -> 1; matrix products, arithmetic and copies ran while one was open for 9% -> 5% of each run, Pallas kernels for 0% -> 74%
where the time goes in v1:
time: 136 us
  Pallas kernels  100 us (74%)
  between operations  14.3 us (11%)
  local copies, waits for them, and re-layouts  6.84 us (5%)
  starting transfers between devices  6.2 us (5%)
  other arithmetic  3.79 us (3%)
  matrix products  3.76 us (3%)
    pallas_call x1, Pallas kernels, expert_mix_of(): pl.pallas_call(functools.partial(expert_kernel, (planes, ranks, sides, pe...  100 us
    ppermute x1, starting transfers between devices, extended(): lax.ppermute(tail, axis, [(i, (i + 1) % count) for i in range(ends)])  4.87 us
    unnamed x12, local copies, waits for them, and re-layouts  3.15 us
  transfers between devices with their start and end apart: 3, of which 1 were waited for; matrix products, arithmetic and copies ran while one was open for 5% of the time, Pallas kernels for 74%

profile of v1, /device:TPU:0, one launch (start us, length us, event | category | flops | bytes accessed | tf_op | source)
XLA Modules:
  0.0 135.6 jit_solution(6131521813290472709)
XLA Ops:
  7.2 0.0 reduce-scatter.2.cloned.1.call-start
  7.2 1.0 copy.29
  8.2 4.9 %collective-permute-start = (bf16[128,2,128]{2,0,1:T(8,128)(2,1)S(1)}, bf16[128,2,128]{2,0,1:T(8,128)(2,1)S(1)}, u32[]{:S(2)}, u32[]{:S(2)}) collective-permute-start(bf16[128,2,128]{2,0,1:T(8,128)(2,1)S(1)} %get-tuple-element.8), channel_id=1, source_target_pairs={{0,4},{4,8},{8,12},{12,16},{16,20},{20,24},{24,28},{1,5},{5,9},{9,... | collective-permute-start | bytes 196616 | tf_op jit(solution)/shard_map/ppermute | solution.py:26
  13.1 1.3 collective-permute-start.1
  14.4 0.1 iota_add_fusion
  14.5 0.1 fusion.15
  14.6 1.1 copy.35
  15.7 1.2 reshape.145
  17.0 0.7 max.17
  17.7 0.3 fusion.5
  18.0 0.9 fusion.8
  18.9 0.0 collective-permute-done
  19.0 0.3 collective-permute-done.1
  19.3 0.1 pad_maximum_fusion.2
  19.3 0.2 copy.34
  19.5 0.2 copy.36
  19.7 0.1 pad_maximum_fusion
  19.8 1.0 fusion.18
  20.8 0.1 broadcast_maximum_fusion
  20.9 0.4 fusion.1
  21.3 0.1 exponential_add_fusion
  21.4 0.0 copy-start
  21.4 0.7 fusion.4
  22.1 0.0 copy-start.1
  22.1 0.0 copy-start.4
  22.1 0.0 copy-start.2
  22.1 0.0 copy-start.3
  22.2 0.2 copy.40
  22.4 0.3 copy-done
  22.6 2.1 %convolution_convert_fusion = bf16[512,2048]{1,0:T(8,128)(2,1)} fusion(bf16[256,2048]{1,0:T(8,128)(2,1)S(1)} %copy-done, bf16[32,8,4,128]{3,2,1,0:T(4,128)(2,1)S(1)} %bitcast.53), kind=kOutput, calls=%fused_computation.4 | convolution fusion | flops 537919488 | bytes 3407872 | tf_op jit(solution)/shard_map/dot_general | solution.py:487
  24.7 0.0 reduce-scatter.2.cloned.1.call-update
  24.7 0.0 copy-done.1
  24.7 0.0 copy-done.4
  24.8 0.0 copy-done.2
  24.8 0.1 convert_reduce_fusion
  25.0 0.0 copy-done.3
  25.0 0.6 fusion.13.sel_ref
  25.6 0.8 add_convert_fusion.meta_ref
  26.5 100.4 %shard_map.140 = bf16[128,2048]{1,0:T(8,128)(2,1)} custom-call(bf16[128,2048]{1,0:T(8,128)(2,1)} %x_ref.1, f32[1,2048]{1,0:T(1,128)} %bitcast.54, bf16[128,128]{1,0:T(8,128)(2,1)} %fusion.13.sel_ref, bf16[128,128]{1,0:T(8,128)(2,1)} %add_convert_fusion.meta_ref, bf16[2,2048,1024]{2,1,0:T(8,128)(2,1)} %wg_hbm.1, bf16[2,2048,1024]{2,1,0:T(8,128)(2,1)} %wu_hbm.1, ...), custom_call_target="tpu_custom_call" | custom-call | flops 12884901888 | bytes 25165824 | tf_op jit(solution)/shard_map/pallas_call | solution.py:385
  126.9 0.0 reduce-scatter.2.cloned.1.call-done
  126.9 1.9 %copy.58 = bf16[128,2048]{1,0:T(8,128)(2,1)} copy(bf16[128,2048]{1,0:T(8,128)(2,1)} %shard_map.140) | data formatting | bytes 1048576
  (12 shorter events, 0.1 us)
Async XLA Ops:
  7.2 119.7 %reduce-scatter.2.cloned.1.call-start = ((), (), s32[]{:S(2)}) async-start(), calls=%async_computation.1 | async-start | bytes 2621440 | tf_op jit(solution)/shard_map/reduce_scatter | solution.py:486
  8.2 10.7 %collective-permute-start = (bf16[128,2,128]{2,0,1:T(8,128)(2,1)S(1)}, bf16[128,2,128]{2,0,1:T(8,128)(2,1)S(1)}, u32[]{:S(2)}, u32[]{:S(2)}) collective-permute-start(bf16[128,2,128]{2,0,1:T(8,128)(2,1)S(1)} %get-tuple-element.8), channel_id=1, source_target_pairs={{0,4},{4,8},{8,12},{12,16},{16,20},{20,24},{24,28},{1,5},{5,9},{9,... | collective-permute-start | bytes 196616 | tf_op jit(solution)/shard_map/ppermute | solution.py:26
  13.1 6.2 %collective-permute-start.1 = (bf16[128,2,128]{2,0,1:T(8,128)(2,1)S(1)}, bf16[128,2,128]{2,0,1:T(8,128)(2,1)S(1)}, u32[]{:S(2)}, u32[]{:S(2)}) collective-permute-start(bf16[128,2,128]{2,0,1:T(8,128)(2,1)S(1)} %get-tuple-element.9), channel_id=1, source_target_pairs={{4,0},{8,4},{12,8},{16,12},{20,16},{24,20},{28,24},{5,1},{9,5},{13... | collective-permute-start | bytes 196616 | tf_op jit(solution)/shard_map/ppermute | solution.py:28
  21.4 1.2 copy-start
  22.1 2.6 %copy-start.1 = (f32[128,4]{0,1:T(4,128)S(1)}, f32[128,4]{0,1:T(4,128)}, u32[]{:S(2)}) copy-start(f32[128,4]{0,1:T(4,128)} %param.21) | copy-start | bytes 6148
  22.1 2.6 %copy-start.4 = (s32[128]{0:T(128)S(1)}, s32[128]{0:T(128)}, u32[]{:S(2)}) copy-start(s32[128]{0:T(128)} %param.19) | copy-start | bytes 1540
  22.1 2.7 %copy-start.2 = (f32[128,2]{0,1:T(2,128)S(1)}, f32[128,2]{0,1:T(2,128)}, u32[]{:S(2)}) copy-start(f32[128,2]{0,1:T(2,128)} %param.22) | copy-start | bytes 3076
  22.1 2.8 %copy-start.3 = (s32[128,2]{0,1:T(2,128)S(1)}, s32[128,2]{0,1:T(2,128)}, u32[]{:S(2)}) copy-start(s32[128,2]{0,1:T(2,128)} %param.20) | copy-start | bytes 3076
Sparse Core Ops, SparseCore 0:
  24.9 41.5 reduce-scatter.1

commit v2 on v1

--- a/solution.py
+++ b/solution.py
@@ -15,23 +15,6 @@
 masked_score = -1e30
 
 
-def extended(cells, sides, width):
-    for axis, dim in sides:
-        count = lax.axis_size(axis)
-        ends = count - 1
-        head = lax.slice_in_dim(cells, 0, width, axis=dim)
-        tail = lax.slice_in_dim(cells, cells.shape[dim] - width, cells.shape[dim], axis=dim)
-        cells = jnp.concatenate(
-            [
-                lax.ppermute(tail, axis, [(i, (i + 1) % count) for i in range(ends)]),
-                cells,
-                lax.ppermute(head, axis, [((i + 1) % count, i) for i in range(ends)]),
-            ],
-            axis=dim,
-        )
-    return cells
-
-
 MESH = pl.DeviceIdType.MESH
 CORES = 2
 META = 128
@@ -40,9 +23,11 @@
 
 
 def expert_kernel(
-    dims, x_ref, gain_ref, sel_ref, meta_ref, wg_hbm, wu_hbm, wd_hbm, out_ref,
+    dims, x_ref, gain_ref, sel_ref, meta_ref, q_ref, kv_ref, sink_ref, ow_ref,
+    wg_hbm, wu_hbm, wd_hbm, mixed_ref, out_ref,
     wg, wu, wd, sbuf, buf, cbuf, xbuf, hbuf, wrow, pbuf, fb, sb, fin, ret,
     wsem, lsem, zs, zr, gs, gr, ps, pr, fs, fr, ss, sr, bs, br,
+    kvx, att, mp, mq, mr, ks, kr, ms, mt, ns, nt, credit,
 ):
     planes, ranks, rows, per_block = dims
     tokens, width = x_ref.shape
@@ -76,6 +61,9 @@
     friends += [device(g, x_peer(i), y, c) for i in range(1, ranks)]
     friends += [device(g, x, y_peer(j), c) for j in range(1, sides)]
     friends += [device(g, x, y, other)]
+    ep_size = lax.axis_size("ep")
+    after, ahead = lax.rem(ep + 1, ep_size), lax.rem(ep + ep_size - 1, ep_size)
+    friends += [(after, tp), (ahead, tp)]
     for f in friends:
         pl.semaphore_signal(barrier, inc=1, device_id=f, device_id_type=MESH)
 
@@ -106,6 +94,77 @@
     own = pltpu.make_async_copy(sbuf.at[g], buf.at[0, c, x, y], lsem)
     own.start()
     own.wait()
+    seq = q_ref.shape[0]
+    halos = [
+        remote(kv_ref.at[pl.ds(seq - WINDOW, WINDOW)], kvx.at[pl.ds(0, WINDOW)], ks.at[0], kr.at[0], (after, tp)),
+        remote(kv_ref.at[pl.ds(0, WINDOW)], kvx.at[pl.ds(seq + WINDOW, WINDOW)], ks.at[1], kr.at[1], (ahead, tp)),
+    ]
+    kvx[pl.ds(WINDOW, seq), :] = kv_ref[...]
+
+    blocks = seq // WINDOW
+    kv_local = kv_ref.shape[1] // META
+    head_size = META // 2
+    heads = q_ref.shape[1] // head_size
+
+    def attention(n):
+        qi = lax.broadcasted_iota(jnp.int32, (WINDOW, 3 * WINDOW), 0)
+        ki = lax.broadcasted_iota(jnp.int32, (WINDOW, 3 * WINDOW), 1)
+        distance = jnp.abs(ki - WINDOW - qi)
+        place = ki + (ep * seq + (n - 1) * WINDOW)
+        allowed = (distance <= WINDOW) & (place >= 0) & (place < seq * ep_size)
+        apart = distance.astype(jnp.float32)
+        outs = []
+        for h in range(heads):
+            at = h // (heads // kv_local) * META
+            query = q_ref[n * WINDOW : (n + 1) * WINDOW, h * head_size : (h + 1) * head_size]
+            near = kvx[n * WINDOW : (n + 3) * WINDOW, at : at + META]
+            power = (tp * heads + h + 1).astype(jnp.float32) * (-8.0 / HEADS * 0.6931471805599453)
+            slope = jnp.exp(jnp.full((1, 1), power, jnp.float32))
+            scores = lax.dot_general(
+                query, near[:, :head_size], (((1,), (1,)), ((), ())), preferred_element_type=jnp.float32
+            ) * head_size ** (-0.5)
+            scores = jnp.where(allowed, scores - slope * apart, masked_score)
+            sink = sink_ref[:, h : h + 1]
+            top = jnp.maximum(jnp.max(scores, axis=-1, keepdims=True), sink)
+            grown = jnp.exp(scores - top)
+            below = jnp.sum(grown, axis=-1, keepdims=True) + jnp.exp(sink - top)
+            weights = (grown / below).astype(jnp.bfloat16)
+            outs.append(jnp.dot(weights, near[:, head_size:], preferred_element_type=jnp.float32))
+        att[n * WINDOW : (n + 1) * WINDOW, :] = jnp.concatenate(outs, axis=1).astype(jnp.bfloat16)
+
+    def attend_share(k):
+        if k == 0:
+            for cp in halos:
+                cp.wait_recv()
+        for n in range(k * blocks // planes, (k + 1) * blocks // planes):
+            attention(n)
+
+    def mix():
+        @pl.loop(0, width // 256)
+        def _(k):
+            cols = pl.ds(pl.multiple_of(k * 256, 256), 256)
+            got = jnp.dot(att[...], ow_ref[:, cols], preferred_element_type=jnp.float32)
+            mp[:, :, :, cols] = got.astype(jnp.bfloat16).reshape(*mp.shape[:3], 256)
+        return [
+            remote(mp.at[q, other], mq.at[q], ms.at[q], mt.at[q], device(g, x, y, other))
+            for q in range(sides)
+        ]
+
+    def mix_hop(swapped):
+        for q in range(sides):
+            swapped[q].wait_recv()
+            mp[q, c] = (mp[q, c].astype(jnp.float32) + mq[q].astype(jnp.float32)).astype(jnp.bfloat16)
+        return [
+            remote(mp.at[y_peer(j), c], mr.at[j - 1], ns.at[j - 1], nt.at[j - 1], device(g, x, y_peer(j), c))
+            for j in range(1, sides)
+        ]
+
+    def mix_end(moved):
+        total = mp[y, c].astype(jnp.float32)
+        for j, cp in enumerate(moved):
+            cp.wait_recv()
+            total += mr[j].astype(jnp.float32)
+        mixed_ref[...] = total.astype(jnp.bfloat16)
 
     counter = [0]
 
@@ -163,20 +222,14 @@
                 landed(d, other, bx, by)
 
     spread(0)
+    attend_share(0)
     for d in range(1, planes):
         spread(d)
         relay(d - 1)
         if d > 1:
             relay_far(d - 2)
-    relay(planes - 1)
-    relay_far(planes - 2)
-    relay_far(planes - 1)
-    for d in range(planes):
-        complete(d)
-    for cp in sent:
-        cp.wait_send()
-    for cp in loads:
-        cp.wait()
+        attend_share(d)
+    swapped = mix()
 
     count = CORES * ranks * sides
     many = count * per_group
@@ -249,8 +302,10 @@
     pair, first_hop, second_hop, home = {}, {}, {}, {}
 
     def swap_cores(d):
+        if d >= stage:
+            pl.semaphore_wait(credit, 1)
         pair[d] = remote(
-            buf.at[d, other, :, :, :, part], pbuf.at[d], ps.at[d], pr.at[d], device(g, x, y, other)
+            buf.at[d, other, :, :, :, part], pbuf.at[d % stage], ps.at[d], pr.at[d], device(g, x, y, other)
         )
 
     def hop_one(d):
@@ -258,8 +313,10 @@
         for bx in range(ranks):
             for by in range(sides):
                 buf[d, c, bx, by, :, part] = (
-                    buf[d, c, bx, by, :, part].astype(jnp.float32) + pbuf[d, bx, by].astype(jnp.float32)
+                    buf[d, c, bx, by, :, part].astype(jnp.float32) + pbuf[d % stage, bx, by].astype(jnp.float32)
                 ).astype(jnp.bfloat16)
+        if d < planes - stage:
+            pl.semaphore_signal(credit, inc=1, device_id=device(g, x, y, other), device_id_type=MESH)
         first_hop[d] = []
         along_y = d % 2 == 0
         for j in range(1, sides if along_y else ranks):
@@ -306,7 +363,14 @@
     for first in range(0, planes, stage):
         ds = range(first, first + stage)
         before = range(first - stage, first) if first else ()
+        for d in ds:
+            complete(d)
         gather_rows(first)
+        if not first:
+            relay(planes - 1)
+            relay_far(planes - 2)
+            loads[0].wait()
+            loads[1].wait()
         for d in before:
             hop_one(d)
         for e in range(local):
@@ -314,17 +378,27 @@
             if e == 0:
                 for d in before:
                     hop_two(d)
+                if not first:
+                    relay_far(planes - 1)
+                    moved = mix_hop(swapped)
         for d in before:
             go_home(d)
+        if not first:
+            loads[2].wait()
+            for cp in sent:
+                cp.wait_send()
         project(first)
         for d in ds:
             swap_cores(d)
+    mix_end(moved)
     for d in ds:
         hop_one(d)
     for d in ds:
         hop_two(d)
     for d in ds:
         go_home(d)
+    for cp in halos + swapped + moved:
+        cp.wait_send()
     for d in range(planes):
         pair[d].wait_send()
         for cp in first_hop[d] + second_hop[d]:
@@ -342,7 +416,8 @@
     ).astype(jnp.bfloat16)
 
 
-def expert_mix_of(
+def both_of(
+    queries, keys_values, sink_logits, out_weight,
     expert_input, norm_gain, route_group, route_expert, group_logits, expert_logits,
     gate_weight, up_weight, down_weight,
 ):
@@ -382,11 +457,14 @@
     vmem = pl.BlockSpec(memory_space=pltpu.VMEM)
     hbm = pl.BlockSpec(memory_space=pl.ANY)
     rows = 2 * slots
+    seq = queries.shape[0]
+    kv = keys_values.reshape(seq, -1)
+    share = seq // tp_size
     return pl.pallas_call(
         functools.partial(expert_kernel, (planes, ranks, sides, per_block)),
-        out_shape=jax.ShapeDtypeStruct((tokens, width), bf16),
-        in_specs=[vmem] * 4 + [hbm] * 3,
-        out_specs=vmem,
+        out_shape=(jax.ShapeDtypeStruct((share, width), bf16), jax.ShapeDtypeStruct((tokens, width), bf16)),
+        in_specs=[vmem] * 8 + [hbm] * 3,
+        out_specs=(vmem, vmem),
         scratch_shapes=[
             pltpu.VMEM(gate_weight.shape, bf16),
             pltpu.VMEM(up_weight.shape, bf16),
@@ -397,7 +475,7 @@
             pltpu.VMEM((local, rows, width), bf16),
             pltpu.VMEM((local, rows, units), bf16),
             pltpu.VMEM((local, rows, META), jnp.float32),
-            pltpu.VMEM((planes, ranks, sides, per_group, width), bf16),
+            pltpu.VMEM((2, ranks, sides, per_group, width), bf16),
             pltpu.VMEM((planes, wide, most, per_group, width), bf16),
             pltpu.VMEM((planes, wide, per_group, width), bf16),
             pltpu.VMEM((planes, per_group, width), bf16),
@@ -409,6 +487,13 @@
             dma((planes, wide, most)), dma((planes, wide, most)),
             dma((planes, wide)), dma((planes, wide)),
             dma((planes,)), dma((planes,)),
+            pltpu.VMEM((seq + 2 * WINDOW, kv.shape[1]), bf16),
+            pltpu.VMEM(queries.shape, bf16),
+            pltpu.VMEM((sides, CORES, share, width), bf16),
+            pltpu.VMEM((sides, share, width), bf16),
+            pltpu.VMEM((sides - 1, share, width), bf16),
+            dma((2,)), dma((2,)), dma((sides,)), dma((sides,)), dma((sides - 1,)), dma((sides - 1,)),
+            pltpu.SemaphoreType.REGULAR,
         ],
         compiler_params=pltpu.CompilerParams(
             collective_id=0, has_side_effects=True, vmem_limit_bytes=KERNEL_VMEM
@@ -416,54 +501,10 @@
         cost_estimate=pl.CostEstimate(
             flops=6 * 2 * rows * local * width * units, bytes_accessed=6 * local * width * units, transcendentals=0
         ),
-    )(expert_input, norm_gain[None, :], sel, meta.astype(bf16), gate_weight, up_weight, down_weight)
-
-
-KERNEL_VMEM = 66_000_000
-
-
-def attend(queries, keys_values, sink_logits):
-    row_count = queries.shape[0]
-    head_size = keys_values.shape[2] // 2
-    kv_local = keys_values.shape[1]
-    query_local = queries.shape[1] // head_size
-    per_head = query_local // kv_local
-    blocks = row_count // WINDOW
-    padded = extended(keys_values, (("ep", 0),), WINDOW)
-    framed = padded.reshape(blocks + 2, WINDOW, kv_local, 2 * head_size)
-    nearby = jnp.concatenate([framed[:-2], framed[1:-1], framed[2:]], axis=1)
-    grouped = queries.reshape(blocks, WINDOW, kv_local, per_head, head_size)
-    scores = jnp.einsum(
-        "nqhgd,nkhd->nhgqk", grouped, nearby[..., :head_size], preferred_element_type=jnp.float32
-    ) * head_size ** (-0.5)
-    first_row = lax.axis_index("ep") * row_count
-    sequence = row_count * lax.axis_size("ep")
-    query_place = first_row + jnp.arange(row_count, dtype=jnp.int32).reshape(blocks, WINDOW)
-    key_place = (
-        first_row
-        + jnp.arange(blocks, dtype=jnp.int32)[:, None] * WINDOW
-        - WINDOW
-        + jnp.arange(3 * WINDOW, dtype=jnp.int32)[None, :]
-    )
-    distance = jnp.abs(key_place[:, None, :] - query_place[:, :, None])
-    allowed = (
-        (distance <= WINDOW) & (key_place >= 0)[:, None, :] & (key_place < sequence)[:, None, :]
-    )
-    head_ids = lax.axis_index("tp") * query_local + jnp.arange(
-        query_local, dtype=jnp.int32
-    ).reshape(kv_local, per_head)
-    slopes = jnp.exp2(-8.0 * (head_ids + 1).astype(jnp.float32) / HEADS)
-    scores = scores - slopes[None, :, :, None, None] * distance[:, None, None].astype(jnp.float32)
-    scores = jnp.where(allowed[:, None, None], scores, masked_score)
-    sink_column = sink_logits.reshape(kv_local, per_head)[None, :, :, None]
-    highest = jnp.maximum(jnp.max(scores, axis=-1), sink_column)
-    exponent = jnp.exp(scores - highest[..., None])
-    denominator = jnp.sum(exponent, axis=-1) + jnp.exp(sink_column - highest)
-    weights = (exponent / denominator[..., None]).astype(jnp.bfloat16)
-    mixed_part = jnp.einsum(
-        "nhgqk,nkhd->nqhgd", weights, nearby[..., head_size:], preferred_element_type=jnp.float32
-    )
-    return mixed_part.astype(jnp.bfloat16).reshape(row_count, query_local * head_size)
+    )(expert_input, norm_gain[None, :], sel, meta.astype(bf16), queries, kv, sink_logits[None, :], out_weight, gate_weight, up_weight, down_weight)
+
+
+KERNEL_VMEM = 67_043_328
 
 
 def body(
@@ -481,19 +522,11 @@
     up_weight,
     down_weight,
 ):
-    attended = attend(queries, keys_values, sink_logits)
-    segment = attended
-    mixed_rows = lax.psum_scatter(
-        jnp.dot(segment, out_weight, preferred_element_type=jnp.float32).astype(jnp.bfloat16),
-        "tp",
-        scatter_dimension=0,
-        tiled=True,
-    )
-    expert_mix = expert_mix_of(
+    return both_of(
+        queries, keys_values, sink_logits, out_weight,
         expert_input, norm_gain, route_group, route_expert, group_logits, expert_logits,
         gate_weight, up_weight, down_weight,
     )
-    return (mixed_rows, expert_mix)
 
 
 def solution(mesh):

time: 136 us -> 114 us (0.84)
  between operations: 14.3 us -> 0.66 us
  starting transfers between devices: 6.2 us -> 0 us
  matrix products: 3.76 us -> 0 us
  other arithmetic: 3.79 us -> 5.82 us
  Pallas kernels: 100 us -> 102 us
  local copies, waits for them, and re-layouts: 6.84 us -> 5.46 us
    ppermute x2 -> x0, starting transfers between devices: 6.17 us -> none  [the longest x1 4.87 us: extended(): lax.ppermute(tail, axis, [(i, (i + 1) % count) for i in range(ends)])]
    dot_general x3 -> x0, matrix products: 3.76 us -> none  [the longest x1 2.09 us: body(): jnp.dot(segment, out_weight, preferred_element_type=jnp.float32)]
    unnamed x12 -> x3, local copies, waits for them, and re-layouts: 3.15 us -> 5.45 us
    reduce_sum x4 -> x3, other arithmetic: 0.59 us -> 2.23 us  [the longest x1 0.83 us: both_of(): place = route_group * per_group + jnp.sum(same.astype(jnp.int32), axis=0)]
    slice x4 -> x0, local copies, waits for them, and re-layouts: 1.5 us -> none  [the longest x3 1.49 us: attend(): nearby = jnp.concatenate([framed[:-2], framed[1:-1], framed[2:]], axis=1)]
  transfers between devices with their start and end apart: 3 -> 0, of which waited for: 1 -> 0; matrix products, arithmetic and copies ran while one was open for 5% -> 0% of each run, Pallas kernels for 74% -> 0%
where the time goes in v2:
time: 114 us
  Pallas kernels  102 us (89%)
  other arithmetic  5.82 us (5%)
  local copies, waits for them, and re-layouts  5.46 us (5%)
    pallas_call x1, Pallas kernels, both_of(): pl.pallas_call(functools.partial(expert_kernel, (planes, ranks, sides, pe...  102 us
    unnamed x3, local copies, waits for them, and re-layouts  5.45 us

profile of v2, /device:TPU:0, one launch (start us, length us, event | category | flops | bytes accessed | tf_op | source)
XLA Modules:
  0.0 113.6 jit_solution(12370811667482653826)
XLA Ops:
  0.6 0.7 exponential_reduce_fusion.1
  1.3 0.8 convert_reduce_fusion
  2.2 0.7 multiply_add_fusion
  2.8 0.7 exponential_reduce_fusion
  3.5 0.7 fusion.2
  4.2 0.8 slice_bitcast_fusion.5
  5.0 0.8 add_convert_fusion.meta_ref
  5.8 0.6 fusion.1.sel_ref
  6.5 1.7 %copy.17 = bf16[64,8,2,128]{3,1,2,0:T(8,128)(2,1)} copy(bf16[64,8,2,128]{3,2,1,0:T(2,128)(2,1)} %bitcast.26) | data formatting | bytes 524288
  8.2 101.7 %shard_map.140 = (bf16[128,2048]{1,0:T(8,128)(2,1)}, bf16[128,2048]{1,0:T(8,128)(2,1)}) custom-call(bf16[128,2048]{1,0:T(8,128)(2,1)} %x_ref.1, f32[1,2048]{1,0:T(1,128)} %bitcast.28, bf16[128,128]{1,0:T(8,128)(2,1)} %fusion.1.sel_ref, bf16[128,128]{1,0:T(8,128)(2,1)} %add_convert_fusion.meta_ref, bf16[512,256]{1,0:T(8,128)(2,1)} %q_ref.1, ...), custom_call_target="tpu_custom_call" | custom-call | flops 12884901888 | bytes 25165824 | tf_op jit(solution)/shard_map/pallas_call | solution.py:463
  109.8 1.9 %copy.20 = bf16[128,2048]{1,0:T(8,128)(2,1)} copy(bf16[128,2048]{1,0:T(8,128)(2,1)} %get-tuple-element.20) | data formatting | bytes 1048576
  111.7 1.9 %copy.21 = bf16[128,2048]{1,0:T(8,128)(2,1)} copy(bf16[128,2048]{1,0:T(8,128)(2,1)} %get-tuple-element.21) | data formatting | bytes 1048576
  (3 shorter events, 0.0 us)
